TPU v7x, 32 devices: a whole 2x2x4 slice. The times are simulated.
32 devices in a mesh: rep: 4 (over z), fs: 4 (over y, x), tp: 2 (over core).
Axes of the slice: x: 2, y: 2, z: 4, core: 2. Of those that a mesh axis runs over, the one named last changes fastest.
Arguments:
- tokens_in: bfloat16 [3072, 1024], P(('rep', 'fs', 'tp')), may hold values from -6 to 6
- out_grad: bfloat16 [3072, 1024], P(('rep', 'fs', 'tp')), may hold values from -6 to 6
- gate_weight: bfloat16 [1024, 2816], P('fs', 'tp'), may hold values from -0.1875 to 0.1875
- up_weight: bfloat16 [1024, 2816], P('fs', 'tp'), may hold values from -0.1875 to 0.1875
- down_weight: bfloat16 [2816, 1024], P('tp', 'fs'), may hold values from -0.109375 to 0.109375
Outputs:
- grad_in: bfloat16 [3072, 1024], P(('rep', 'fs', 'tp'))
- grad_gate_w: float32 [1024, 2816], P('fs', 'tp')
- grad_up_w: float32 [1024, 2816], P('fs', 'tp')
- grad_down_w: float32 [2816, 1024], P('tp', 'fs')
All inputs are finite; a program needn't handle non-finite values.
Results may differ from a plain program's by a relative error of at most 0.02.
Values may be sent and summed in bfloat16 or wider, within the bound.
A program may use at most 64 MiB of HBM per device.

v0:
```python
import jax
import jax.numpy as jnp
from jax import lax
from jax.sharding import PartitionSpec as P


def contract_last(left, right):
    return lax.dot_general(
        left, right, (((1,), (1,)), ((), ())), preferred_element_type=jnp.float32
    )


def contract_first(left, right):
    return lax.dot_general(
        left, right, (((0,), (0,)), ((), ())), preferred_element_type=jnp.float32
    )


def body(tokens_in, out_grad, gate_weight, up_weight, down_weight):
    replicas = lax.axis_size("rep")
    shards = lax.axis_size("fs")
    columns = lax.axis_size("tp")
    local_rows = tokens_in.shape[0]
    hidden_cols = gate_weight.shape[1]
    factor = (local_rows * replicas * shards * columns) ** (-0.5)
    part = hidden_cols // replicas
    offset = lax.axis_index("rep") * part
    pieces = jnp.stack(
        [
            lax.dynamic_slice_in_dim(gate_weight, offset, part, 1).T,
            lax.dynamic_slice_in_dim(up_weight, offset, part, 1).T,
            lax.dynamic_slice_in_dim(down_weight, offset, part, 0),
        ]
    )
    full = lax.all_gather(pieces, "fs", axis=2, tiled=True)
    gate_full, up_full, down_full = (full[0], full[1], full[2])
    both = lax.all_gather(jnp.stack([tokens_in, out_grad]), ("rep", "tp"), axis=1, tiled=True)
    tokens_all, grads_all = (both[0], both[1])
    gate = contract_last(tokens_all, gate_full).astype(jnp.bfloat16)
    up_proj = contract_last(tokens_all, up_full).astype(jnp.bfloat16)
    gate_wide = gate.astype(jnp.float32)
    up_wide = up_proj.astype(jnp.float32)
    sigmoid = jax.nn.sigmoid(gate_wide)
    activated = gate_wide * sigmoid
    hidden = (activated * up_wide).astype(jnp.bfloat16)
    grad_hidden = contract_last(grads_all, down_full).astype(jnp.bfloat16)
    grad_wide = grad_hidden.astype(jnp.float32)
    grad_gate = (grad_wide * up_wide * sigmoid * (1.0 + gate_wide * (1.0 - sigmoid))).astype(
        jnp.bfloat16
    )
    grad_up = (grad_wide * activated).astype(jnp.bfloat16)
    weights = factor * jnp.stack(
        [
            contract_first(grad_gate, tokens_all),
            contract_first(grad_up, tokens_all),
            contract_first(hidden, grads_all),
        ]
    )
    owned = lax.psum_scatter(weights.astype(jnp.bfloat16), "fs", scatter_dimension=2, tiled=True)
    summed = lax.all_gather(owned, "rep", axis=1, tiled=True).astype(jnp.float32)
    partial = jnp.dot(grad_gate, gate_full, preferred_element_type=jnp.float32) + jnp.dot(
        grad_up, up_full, preferred_element_type=jnp.float32
    )
    grad_in = lax.psum_scatter(
        partial.astype(jnp.bfloat16), ("rep", "tp"), scatter_dimension=0, tiled=True
    )
    return (grad_in, summed[0].T, summed[1].T, summed[2])


def solution(mesh):
    placed = (
        P(("rep", "fs", "tp"), None),
        P(("rep", "fs", "tp"), None),
        P("fs", "tp"),
        P("fs", "tp"),
        P("tp", "fs"),
    )
    return jax.shard_map(
        body,
        mesh=mesh,
        in_specs=placed,
        out_specs=(P(("rep", "fs", "tp"), None), P("fs", "tp"), P("fs", "tp"), P("tp", "fs")),
        check_vma=False,
    )
```

profile of v0, /device:TPU:0, one launch (start us, length us, event | category | flops | bytes accessed | tf_op | source)
XLA Modules:
  0.0 225.2 jit_solution(11727370553388090820)
XLA Ops:
  7.2 0.0 copy-start
  7.2 0.0 all-gather.6.cloned.1.call-start
  7.2 1.0 copy-done
  8.3 0.0 copy-start.1
  8.3 0.0 copy-start.2
  8.3 1.3 constant_dynamic-slice_fusion
  9.6 0.1 copy.16
  9.8 0.1 copy.15
  9.9 0.9 pad_maximum_fusion
  10.8 0.0 all-gather.6.cloned.1.call-update
  10.8 0.0 all-gather.4.cloned.1.call-start
  10.8 0.0 copy-done.1
  10.8 0.0 copy-done.2
  10.9 0.8 pad_maximum_fusion.1
  11.6 0.0 all-gather.4.cloned.1.call-update
  11.7 0.0 reduce-scatter.5.cloned.1.call-start
  11.7 37.5 %all-gather.6.cloned.1.call-done = bf16[3,352,1024]{2,1,0:T(8,128)(2,1)} async-done(((bf16[3,352,256]{2,1,0:T(8,128)(2,1)}), bf16[3,352,1024]{2,1,0:T(8,128)(2,1)}) %all-gather.6.cloned.1.call-update) | async-done | bytes 2162704 | tf_op jit(solution)/shard_map/all_gather | solution.py:35
  49.2 40.4 %all-gather.4.cloned.1.call-done = bf16[2,768,1024]{2,1,0:T(8,128)(2,1)} async-done(((bf16[2,96,1024]{2,1,0:T(8,128)(2,1)}), bf16[2,768,1024]{2,1,0:T(8,128)(2,1)}) %all-gather.4.cloned.1.call-update) | async-done | bytes 3145744 | tf_op jit(solution)/shard_map/all_gather | solution.py:37
  89.7 0.0 copy-start.3
  89.7 2.5 %convolution_convert_fusion.1 = bf16[768,352]{0,1:T(8,128)(2,1)S(1)} fusion(bf16[2,768,1024]{2,1,0:T(8,128)(2,1)} %all-gather.4.cloned.1.call-done, bf16[3,352,1024]{2,1,0:T(8,128)(2,1)} %all-gather.6.cloned.1.call-done), kind=kOutput, calls=%fused_computation.20 | convolution fusion | flops 553918464 | bytes 2834432 | tf_op jit(solution)/shard_map/dot_general | solution.py:8
  92.2 0.1 copy-done.3
  92.2 0.0 copy-start.7
  92.2 0.0 copy-start.4
  92.3 2.2 fusion.2
  94.4 0.0 copy-done.4
  94.4 0.8 convolution_convert_fusion
  95.2 0.0 copy-start.5
  95.2 0.8 convolution_bitcast_fusion
  96.1 0.9 convolution_bitcast_fusion.1
  96.9 0.0 copy-done.7
  96.9 0.0 copy-done.5
  96.9 1.0 convolution_bitcast_fusion.2
  98.0 2.0 fusion
  99.9 0.0 reduce-scatter.5.cloned.1.call-update
  100.0 0.0 all-gather.8.cloned.1.call-start
  100.0 34.8 %reduce-scatter.5.cloned.1.call-done = bf16[3,352,256]{2,1,0:T(8,128)(2,1)} async-done(((bf16[3,352,1024]{2,1,0:T(8,128)(2,1)}), bf16[3,352,256]{2,1,0:T(8,128)(2,1)}) %reduce-scatter.5.cloned.1.call-update) | async-done | bytes 540688 | tf_op jit(solution)/shard_map/reduce_scatter | solution.py:59
  134.8 0.0 all-gather.8.cloned.1.call-update
  134.8 0.0 reduce-scatter.3.cloned.1.call-start
  134.8 0.0 copy-start.6
  134.8 2.5 %fusion.12 = f32[768,1024]{1,0:T(8,128)S(1)} fusion(bf16[3,352,1024]{2,1,0:T(8,128)(2,1)S(1)} %copy-done.4, bf16[768,352]{0,1:T(8,128)(2,1)} %copy-done.7, bf16[768,352]{0,1:T(8,128)(2,1)S(1)} %fusion.2, bf16[768,352]{0,1:T(8,128)(2,1)} %copy-done.5), kind=kOutput, calls=%fused_computation.33 | convolution fusion | flops 557162496 | bytes 5488640 | tf_op jit(solution)/shard_map/dot_general | solution.py:61
  137.4 0.0 copy-done.6
  137.4 2.3 %add_convert_fusion = bf16[768,1024]{1,0:T(8,128)(2,1)} fusion(f32[768,1024]{1,0:T(8,128)S(1)} %fusion.12, bf16[3,352,1024]{2,1,0:T(8,128)(2,1)S(1)} %copy-done.4, bf16[768,352]{0,1:T(8,128)(2,1)S(1)} %fusion.2, bf16[768,352]{0,1:T(8,128)(2,1)S(1)} %copy-done.6), kind=kOutput, calls=%fused_computation.2 | convolution fusion | flops 557383680 | bytes 6520832 | tf_op jit(solution)/shard_map/dot_general | solution.py:61
  139.7 0.0 reduce-scatter.3.cloned.1.call-update
  139.7 43.2 %all-gather.8.cloned.1.call-done = bf16[3,1408,256]{2,1,0:T(8,128)(2,1)} async-done(((bf16[3,352,256]{2,1,0:T(8,128)(2,1)}), bf16[3,1408,256]{2,1,0:T(8,128)(2,1)}) %all-gather.8.cloned.1.call-update) | async-done | bytes 2162704 | tf_op jit(solution)/shard_map/all_gather | solution.py:60
  183.0 2.0 convert_element_type.47
  185.0 2.0 slice_bitcast_fusion.2
  186.9 2.9 %copy.13 = f32[256,1408]{1,0:T(8,128)} copy(f32[256,1408]{0,1:T(8,128)} %get-tuple-element.14) | data formatting | bytes 2883584
  189.8 1.5 copy.14
  191.4 27.3 %reduce-scatter.3.cloned.1.call-done = bf16[96,1024]{1,0:T(8,128)(2,1)} async-done(((bf16[768,1024]{1,0:T(8,128)(2,1)}), bf16[96,1024]{1,0:T(8,128)(2,1)}) %reduce-scatter.3.cloned.1.call-update) | async-done | bytes 196624 | tf_op jit(solution)/shard_map/reduce_scatter | solution.py:64
  (1 shorter events, 0.0 us)
Async XLA Ops:
  7.2 1.1 copy-start
  7.2 42.1 %all-gather.6.cloned.1.call-start = ((), (), s32[]{:S(2)}) async-start(), calls=%async_computation.3 | async-start | bytes 2703360 | tf_op jit(solution)/shard_map/all_gather | solution.py:35
  8.3 2.5 %copy-start.1 = (bf16[96,1024]{1,0:T(8,128)(2,1)S(1)}, bf16[96,1024]{1,0:T(8,128)(2,1)}, u32[]{:S(2)}) copy-start(bf16[96,1024]{1,0:T(8,128)(2,1)} %param.6) | copy-start | bytes 589828
  8.3 2.5 %copy-start.2 = (bf16[96,1024]{1,0:T(8,128)(2,1)S(1)}, bf16[96,1024]{1,0:T(8,128)(2,1)}, u32[]{:S(2)}) copy-start(bf16[96,1024]{1,0:T(8,128)(2,1)} %param.5) | copy-start | bytes 589828
  10.8 78.9 %all-gather.4.cloned.1.call-start = ((), (), s32[]{:S(2)}) async-start(), calls=%async_computation.2 | async-start | bytes 3538944 | tf_op jit(solution)/shard_map/all_gather | solution.py:37
  11.7 123.1 %reduce-scatter.5.cloned.1.call-start = ((), (), s32[]{:S(2)}) async-start(), calls=%async_computation.5 | async-start | bytes 2703360 | tf_op jit(solution)/shard_map/reduce_scatter | solution.py:59
  89.7 2.6 %copy-start.3 = (bf16[2,768,1024]{2,1,0:T(8,128)(2,1)S(1)}, bf16[2,768,1024]{2,1,0:T(8,128)(2,1)}, u32[]{:S(2)}) copy-start(bf16[2,768,1024]{2,1,0:T(8,128)(2,1)} %all-gather.4.cloned.1.call-done) | copy-start | bytes 9437188
  92.2 4.7 %copy-start.7 = (bf16[768,352]{0,1:T(8,128)(2,1)}, bf16[768,352]{0,1:T(8,128)(2,1)S(1)}, u32[]{:S(2)}) copy-start(bf16[768,352]{0,1:T(8,128)(2,1)S(1)} %convolution_convert_fusion.1) | copy-start | bytes 1622020
  92.2 2.2 copy-start.4
  95.2 1.7 copy-start.5
  100.0 83.0 %all-gather.8.cloned.1.call-start = ((), (), s32[]{:S(2)}) async-start(), calls=%async_computation.6 | async-start | bytes 2703360 | tf_op jit(solution)/shard_map/all_gather | solution.py:60
  134.8 83.8 %reduce-scatter.3.cloned.1.call-start = ((), (), s32[]{:S(2)}) async-start(), calls=%async_computation.4 | async-start | bytes 1769472 | tf_op jit(solution)/shard_map/reduce_scatter | solution.py:64
  134.8 2.6 %copy-start.6 = (bf16[768,352]{0,1:T(8,128)(2,1)S(1)}, bf16[768,352]{0,1:T(8,128)(2,1)}, u32[]{:S(2)}) copy-start(bf16[768,352]{0,1:T(8,128)(2,1)} %copy-done.5) | copy-start | bytes 1622020
Sparse Core Ops, SparseCore 0:
  10.9 38.2 all-gather.5
  51.4 38.1 all-gather.3
  100.1 34.6 reduce-scatter.4
  136.2 46.7 all-gather.7
  185.7 32.8 reduce-scatter.2
where the time goes:
time: 225 us
  waiting for transfers between devices  183 us (81%)
  between operations  13.9 us (6%)
  matrix products  13 us (6%)
  local copies, waits for them, and re-layouts  9.14 us (4%)
  other arithmetic  5.58 us (2%)
    all_gather x1, waiting for transfers between devices, body(): lax.all_gather(owned, 'rep', axis=1, tiled=True).astype(jnp.float32)  43.2 us
    all_gather x1, waiting for transfers between devices, body(): lax.all_gather(jnp.stack([tokens_in, out_grad]), ('rep', 'tp'), axis=1, t...  40.4 us
    all_gather x1, waiting for transfers between devices, body(): full = lax.all_gather(pieces, 'fs', axis=2, tiled=True)  37.5 us
    reduce_scatter x1, waiting for transfers between devices, body(): lax.psum_scatter(weights.astype(jnp.bfloat16), 'fs', scatter_dimension=2,...  34.8 us
    reduce_scatter x1, waiting for transfers between devices, body(): lax.psum_scatter(partial.astype(jnp.bfloat16), ('rep', 'tp'), scatter_dim...  27.3 us
    unnamed x20, local copies, waits for them, and re-layouts  5.87 us
    dot_general x3, matrix products, contract_last(): lax.dot_general(left, right, (((1,), (1,)), ((), ())), preferred_element_...  5.44 us
  transfers between devices with their start and end apart: 5, of which 5 were waited for; matrix products, arithmetic and copies ran while one was open for 6% of the time, Pallas kernels for 0%

commit v1 on v0

--- a/solution.py
+++ b/solution.py
@@ -17,6 +17,10 @@
 
 
 def body(tokens_in, out_grad, gate_weight, up_weight, down_weight):
+
+    def proceed_heads_now(axis_tag, dimension_no, xs):
+        return jnp.concatenate(lax.all_gather(xs, axis_name=axis_tag), dimension_no)
+
     replicas = lax.axis_size("rep")
     shards = lax.axis_size("fs")
     columns = lax.axis_size("tp")
@@ -32,7 +36,7 @@
             lax.dynamic_slice_in_dim(down_weight, offset, part, 0),
         ]
     )
-    full = lax.all_gather(pieces, "fs", axis=2, tiled=True)
+    full = proceed_heads_now("fs", 2, pieces)
     gate_full, up_full, down_full = (full[0], full[1], full[2])
     both = lax.all_gather(jnp.stack([tokens_in, out_grad]), ("rep", "tp"), axis=1, tiled=True)
     tokens_all, grads_all = (both[0], both[1])

time: 225 us -> 224 us (level)
  local copies, waits for them, and re-layouts: 9.14 us -> 13.5 us
  waiting for transfers between devices: 183 us -> 179 us
    all_gather x1, waiting for transfers between devices: 40.4 us -> 36 us  [body(): lax.all_gather(jnp.stack([tokens_in, out_grad]), ('rep', 'tp'), axis=1, t...]
    all_gather x0 -> x1, local copies, waits for them, and re-layouts: none -> 3.28 us  [proceed_heads_now(): return jnp.concatenate(lax.all_gather(xs, axis_name=axis_tag), dimension_no)]
    unnamed x20 -> x17, local copies, waits for them, and re-layouts: 5.87 us -> 6.2 us
  transfers between devices with their start and end apart: 5 -> 5, of which waited for: 5 -> 5; matrix products, arithmetic and copies ran while one was open for 6% -> 8% of each run, Pallas kernels for 0% -> 0%
where the time goes in v1:
time: 224 us
  waiting for transfers between devices  179 us (80%)
  between operations  14 us (6%)
  local copies, waits for them, and re-layouts  13.5 us (6%)
  matrix products  11.2 us (5%)
  other arithmetic  5.58 us (2%)
    all_gather x1, waiting for transfers between devices, body(): lax.all_gather(owned, 'rep', axis=1, tiled=True).astype(jnp.float32)  43.5 us
    all_gather x1, waiting for transfers between devices, proceed_heads_now(): return jnp.concatenate(lax.all_gather(xs, axis_name=axis_tag), dimension_no)  37.7 us
    all_gather x1, waiting for transfers between devices, body(): lax.all_gather(jnp.stack([tokens_in, out_grad]), ('rep', 'tp'), axis=1, t...  36 us
    reduce_scatter x1, waiting for transfers between devices, body(): lax.psum_scatter(weights.astype(jnp.bfloat16), 'fs', scatter_dimension=2,...  34.7 us
    reduce_scatter x1, waiting for transfers between devices, body(): lax.psum_scatter(partial.astype(jnp.bfloat16), ('rep', 'tp'), scatter_dim...  27.3 us
    unnamed x17, local copies, waits for them, and re-layouts  6.2 us
  transfers between devices with their start and end apart: 5, of which 5 were waited for; matrix products, arithmetic and copies ran while one was open for 8% of the time, Pallas kernels for 0%

profile of v1, /device:TPU:0, one launch (start us, length us, event | category | flops | bytes accessed | tf_op | source)
XLA Modules:
  0.0 223.7 jit_solution(18158454545901701577)
XLA Ops:
  7.2 0.0 copy-start
  7.2 0.0 all-gather.9.cloned.1.call-start
  7.2 1.0 copy-done
  8.3 0.0 copy-start.1
  8.3 0.0 copy-start.2
  8.3 1.3 constant_dynamic-slice_fusion
  9.6 0.1 copy.26
  9.8 0.1 copy.25
  9.9 0.9 pad_maximum_fusion
  10.8 0.0 all-gather.9.cloned.1.call-update
  10.8 0.0 all-gather.5.cloned.1.call-start
  10.8 0.0 copy-done.1
  10.8 0.0 copy-done.2
  10.9 0.8 pad_maximum_fusion.1
  11.6 0.0 all-gather.5.cloned.1.call-update
  11.7 0.0 reduce-scatter.5.cloned.1.call-start
  11.7 37.7 %all-gather.9.cloned.1.call-done = bf16[12,352,256]{2,1,0:T(8,128)(2,1)} async-done(((bf16[3,352,256]{2,1,0:T(8,128)(2,1)}), bf16[12,352,256]{2,1,0:T(8,128)(2,1)}) %all-gather.9.cloned.1.call-update) | async-done | bytes 2162704 | tf_op jit(solution)/shard_map/all_gather | solution.py:22
  49.4 3.3 %copy.31 = bf16[4,3,352,256]{3,0,2,1:T(4,128)(2,1)S(1)} copy(bf16[4,3,352,256]{3,2,1,0:T(8,128)(2,1)} %bitcast.60) | data formatting | bytes 4325376 | tf_op jit(solution)/shard_map/all_gather | solution.py:22
  52.7 0.7 fusion.19
  53.4 0.1 copy.29
  53.5 0.1 copy.28
  53.7 0.1 copy.27
  53.8 36.0 %all-gather.5.cloned.1.call-done = bf16[2,768,1024]{2,1,0:T(8,128)(2,1)} async-done(((bf16[2,96,1024]{2,1,0:T(8,128)(2,1)}), bf16[2,768,1024]{2,1,0:T(8,128)(2,1)}) %all-gather.5.cloned.1.call-update) | async-done | bytes 3145744 | tf_op jit(solution)/shard_map/all_gather | solution.py:41
  89.8 0.0 copy-start.3
  89.8 2.3 %convolution_convert_fusion.1 = bf16[768,352]{0,1:T(8,128)(2,1)S(1)} fusion(bf16[352,1024]{1,0:T(8,128)(2,1)S(1)} %bitcast.61, bf16[2,768,1024]{2,1,0:T(8,128)(2,1)} %all-gather.5.cloned.1.call-done), kind=kOutput, calls=%fused_computation.21 | convolution fusion | flops 553918464 | bytes 2834432 | tf_op jit(solution)/shard_map/dot_general | solution.py:8
  92.1 0.0 copy-start.4
  92.1 0.0 copy-done.3
  92.2 0.8 fusion.2
  93.0 0.8 convolution_convert_fusion
  93.8 0.8 convolution_bitcast_fusion
  94.6 0.9 convolution_bitcast_fusion.1
  95.5 0.0 copy-done.4
  95.5 1.0 convolution_bitcast_fusion.2
  96.5 2.0 fusion
  98.5 0.0 reduce-scatter.5.cloned.1.call-update
  98.5 0.0 all-gather.7.cloned.1.call-start
  98.6 34.7 %reduce-scatter.5.cloned.1.call-done = bf16[3,352,256]{2,1,0:T(8,128)(2,1)} async-done(((bf16[3,352,1024]{2,1,0:T(8,128)(2,1)}), bf16[3,352,256]{2,1,0:T(8,128)(2,1)}) %reduce-scatter.5.cloned.1.call-update) | async-done | bytes 540688 | tf_op jit(solution)/shard_map/reduce_scatter | solution.py:63
  133.3 0.0 all-gather.7.cloned.1.call-update
  133.3 0.0 reduce-scatter.3.cloned.1.call-start
  133.4 2.3 %fusion.17 = f32[768,1024]{1,0:T(8,128)S(1)} fusion(bf16[352,1024]{1,0:T(8,128)(2,1)S(1)} %bitcast.64, bf16[768,352]{0,1:T(8,128)(2,1)} %copy-done.4, bf16[768,352]{0,1:T(8,128)(2,1)S(1)} %fusion.2, bf16[768,352]{0,1:T(8,128)(2,1)S(1)} %convolution_convert_fusion), kind=kOutput, calls=%fused_computation.37 | convolution fusion | flops 557162496 | bytes 5488640 | tf_op jit(solution)/shard_map/dot_general | solution.py:65
  135.7 2.3 %add_convert_fusion = bf16[768,1024]{1,0:T(8,128)(2,1)} fusion(f32[768,1024]{1,0:T(8,128)S(1)} %fusion.17, bf16[352,1024]{1,0:T(8,128)(2,1)S(1)} %bitcast.62, bf16[768,352]{0,1:T(8,128)(2,1)S(1)} %fusion.2, bf16[768,352]{0,1:T(8,128)(2,1)S(1)} %convolution_convert_fusion), kind=kOutput, calls=%fused_computation.2 | convolution fusion | flops 557383680 | bytes 6520832 | tf_op jit(solution)/shard_map/dot_general | solution.py:65
  138.0 0.0 reduce-scatter.3.cloned.1.call-update
  138.0 43.5 %all-gather.7.cloned.1.call-done = bf16[3,1408,256]{2,1,0:T(8,128)(2,1)} async-done(((bf16[3,352,256]{2,1,0:T(8,128)(2,1)}), bf16[3,1408,256]{2,1,0:T(8,128)(2,1)}) %all-gather.7.cloned.1.call-update) | async-done | bytes 2162704 | tf_op jit(solution)/shard_map/all_gather | solution.py:64
  181.5 2.0 convert_element_type.47
  183.5 2.0 slice_bitcast_fusion.2
  185.4 2.9 %copy.23 = f32[256,1408]{1,0:T(8,128)} copy(f32[256,1408]{0,1:T(8,128)} %get-tuple-element.22) | data formatting | bytes 2883584
  188.3 1.5 copy.24
  189.9 27.3 %reduce-scatter.3.cloned.1.call-done = bf16[96,1024]{1,0:T(8,128)(2,1)} async-done(((bf16[768,1024]{1,0:T(8,128)(2,1)}), bf16[96,1024]{1,0:T(8,128)(2,1)}) %reduce-scatter.3.cloned.1.call-update) | async-done | bytes 196624 | tf_op jit(solution)/shard_map/reduce_scatter | solution.py:68
  (1 shorter events, 0.0 us)
Async XLA Ops:
  7.2 1.1 copy-start
  7.2 42.2 %all-gather.9.cloned.1.call-start = ((), (), s32[]{:S(2)}) async-start(), calls=%async_computation.6 | async-start | bytes 2703360 | tf_op jit(solution)/shard_map/all_gather | solution.py:22
  8.3 2.5 %copy-start.1 = (bf16[96,1024]{1,0:T(8,128)(2,1)S(1)}, bf16[96,1024]{1,0:T(8,128)(2,1)}, u32[]{:S(2)}) copy-start(bf16[96,1024]{1,0:T(8,128)(2,1)} %param.6) | copy-start | bytes 589828
  8.3 2.5 %copy-start.2 = (bf16[96,1024]{1,0:T(8,128)(2,1)S(1)}, bf16[96,1024]{1,0:T(8,128)(2,1)}, u32[]{:S(2)}) copy-start(bf16[96,1024]{1,0:T(8,128)(2,1)} %param.5) | copy-start | bytes 589828
  10.8 79.0 %all-gather.5.cloned.1.call-start = ((), (), s32[]{:S(2)}) async-start(), calls=%async_computation.2 | async-start | bytes 3538944 | tf_op jit(solution)/shard_map/all_gather | solution.py:41
  11.7 121.6 %reduce-scatter.5.cloned.1.call-start = ((), (), s32[]{:S(2)}) async-start(), calls=%async_computation.4 | async-start | bytes 2703360 | tf_op jit(solution)/shard_map/reduce_scatter | solution.py:63
  89.8 2.4 %copy-start.3 = (bf16[2,768,1024]{2,1,0:T(8,128)(2,1)S(1)}, bf16[2,768,1024]{2,1,0:T(8,128)(2,1)}, u32[]{:S(2)}) copy-start(bf16[2,768,1024]{2,1,0:T(8,128)(2,1)} %all-gather.5.cloned.1.call-done) | copy-start | bytes 9437188
  92.1 3.3 %copy-start.4 = (bf16[768,352]{0,1:T(8,128)(2,1)}, bf16[768,352]{0,1:T(8,128)(2,1)S(1)}, u32[]{:S(2)}) copy-start(bf16[768,352]{0,1:T(8,128)(2,1)S(1)} %convolution_convert_fusion.1) | copy-start | bytes 1622020
  98.5 83.0 %all-gather.7.cloned.1.call-start = ((), (), s32[]{:S(2)}) async-start(), calls=%async_computation.5 | async-start | bytes 2703360 | tf_op jit(solution)/shard_map/all_gather | solution.py:64
  133.3 83.9 %reduce-scatter.3.cloned.1.call-start = ((), (), s32[]{:S(2)}) async-start(), calls=%async_computation.3 | async-start | bytes 1769472 | tf_op jit(solution)/shard_map/reduce_scatter | solution.py:68
Sparse Core Ops, SparseCore 0:
  10.9 38.4 all-gather.8
  51.6 38.1 all-gather.4
  98.6 34.6 reduce-scatter.4
  134.7 46.7 all-gather.6
  184.2 32.9 reduce-scatter.2
